TPU v7x, 32 devices: a whole 2x2x4 slice. The times are simulated.
32 devices in a mesh: ep: 8 (over z, y), tp: 4 (over x, core).
Axes of the slice: x: 2, y: 2, z: 4, core: 2. Of those that a mesh axis runs over, the one named last changes fastest.
Arguments:
- hidden: bfloat16 [256, 2048], P('ep')
- norm_gains: float32 [4, 2048], replicated, may hold values from 0.1 to 1.9
- w_query: bfloat16 [2048, 1024], P(None, 'tp'), may hold values from -0.125 to 0.125
- w_key: bfloat16 [2048, 1024], P(None, 'tp'), may hold values from -0.125 to 0.125
- w_value: bfloat16 [2048, 1024], P(None, 'tp'), may hold values from -0.125 to 0.125
- w_outgate: bfloat16 [2048, 1024], P(None, 'tp'), may hold values from -0.125 to 0.125
- w_input_gate: bfloat16 [2048, 8], replicated, may hold values from -0.125 to 0.125
- w_forget_gate: bfloat16 [2048, 8], replicated, may hold values from -0.125 to 0.125
- forget_bias: float32 [8], replicated, may hold values from -1 to 4
- w_mix_out: bfloat16 [1024, 2048], P('tp')
- state_matrix: float32 [256, 8, 128, 128], P('ep', 'tp'), may hold values from -0.6 to 0.6
- state_norm: float32 [256, 8, 128], P('ep', 'tp'), may hold values from -0.6 to 0.6
- state_max: float32 [256, 8], P('ep', 'tp'), may hold values from -4 to 4
- routes: int32 [256, 2], P('ep'), may hold values from 0 to 7, all different within a row; in each aligned block of 32 rows (0 to 31, 32 to 63, ...) at most 16 rows name the same one
- route_scores: float32 [256, 2], P('ep'), may hold values from 0.1 to 1
- expert_gate: bfloat16 [8, 2048, 3584], P('ep', None, 'tp'), may hold values from -0.125 to 0.125
- expert_up: bfloat16 [8, 2048, 3584], P('ep', None, 'tp'), may hold values from -0.125 to 0.125
- expert_down: bfloat16 [8, 3584, 2048], P('ep', 'tp')
- dense_gate: bfloat16 [2048, 5632], P('tp', 'ep'), may hold values from -0.125 to 0.125
- dense_up: bfloat16 [2048, 5632], P('tp', 'ep'), may hold values from -0.125 to 0.125
- dense_down: bfloat16 [5632, 2048], P('ep', 'tp')
- dense_mix: float32 [2048], replicated, may hold values from -0.25 to 0.25
Outputs:
- new_hidden: bfloat16 [256, 2048], P('ep', 'tp')
- new_matrix: float32 [256, 8, 128, 128], P('ep', 'tp')
- new_norm: float32 [256, 8, 128], P('ep', 'tp')
- new_max: float32 [256, 8], P('ep', 'tp')
Inputs may be any that keep to these rules, and one draw needn't show every extreme that they name: `routes`: each row names 2 different experts. Among the rows of one index of ep (an aligned block of 32 rows) no expert is named by more than 16 rows, and in every draw some expert is named by exactly 16 rows of some block.
All inputs are finite; a program needn't handle non-finite values.
Results may differ from a plain program's by a relative error of at most 0.02.
Values may be sent and summed in bfloat16 or wider, within the bound.
No kernel may reach another device: no remote copies, remote signals or barrier semaphores. Data moves between devices by JAX's collectives and lax.ppermute only.
A program may use at most 128 MiB of HBM per device.

v0:
```python
import jax
import jax.numpy as jnp
from jax import lax
from jax.sharding import PartitionSpec as P

EPS = 1e-06


def settle(values):
    return lax.optimization_barrier(values.astype(jnp.bfloat16)).astype(jnp.float32)


def local(
    hidden,
    norm_gains,
    w_query,
    w_key,
    w_value,
    w_outgate,
    w_input_gate,
    w_forget_gate,
    forget_bias,
    w_mix_out,
    state_matrix,
    state_norm,
    state_max,
    routes,
    route_scores,
    expert_gate,
    expert_up,
    expert_down,
    dense_gate,
    dense_up,
    dense_down,
    dense_mix,
):
    tp_count = lax.axis_size("tp")
    ep_count = lax.axis_size("ep")
    tp_place = lax.axis_index("tp")
    seq_local, width = hidden.shape
    heads_local = state_matrix.shape[1]
    head_width = state_matrix.shape[2]
    part_width = width // tp_count
    feature_first = tp_place * part_width
    start_f = hidden.astype(jnp.float32)
    normed_in = (
        start_f
        * lax.rsqrt(jnp.mean(start_f * start_f, axis=-1, keepdims=True) + EPS)
        * norm_gains[0]
    ).astype(jnp.bfloat16)
    query_f = jnp.dot(normed_in, w_query, preferred_element_type=jnp.float32)
    key_f = jnp.dot(normed_in, w_key, preferred_element_type=jnp.float32)
    value_f = jnp.dot(normed_in, w_value, preferred_element_type=jnp.float32)
    gate_f = jnp.dot(normed_in, w_outgate, preferred_element_type=jnp.float32)
    head_first = tp_place * heads_local
    input_weight = lax.dynamic_slice_in_dim(w_input_gate, head_first, heads_local, 1)
    forget_weight = lax.dynamic_slice_in_dim(w_forget_gate, head_first, heads_local, 1)
    forget_local = lax.dynamic_slice_in_dim(forget_bias, head_first, heads_local, 0)
    in_gate = jnp.dot(normed_in, input_weight, preferred_element_type=jnp.float32)
    log_forget = jax.nn.log_sigmoid(
        jnp.dot(normed_in, forget_weight, preferred_element_type=jnp.float32) + forget_local
    )
    query = settle(query_f).reshape(seq_local, heads_local, head_width)
    keys = settle(key_f).reshape(seq_local, heads_local, head_width) * head_width ** (-0.5)
    values = settle(value_f).reshape(seq_local, heads_local, head_width)
    carried = log_forget + state_max
    new_max = jnp.maximum(carried, in_gate)
    keep = jnp.exp(carried - new_max)
    write = jnp.exp(in_gate - new_max)
    written = write[:, :, None] * keys
    new_matrix = (
        keep[:, :, None, None] * state_matrix + written[:, :, :, None] * values[:, :, None, :]
    )
    new_norm = keep[:, :, None] * state_norm + written
    numer = jnp.einsum("shd,shdv->shv", query, new_matrix)
    denom = jnp.einsum("shd,shd->sh", query, new_norm)
    read = numer / jnp.maximum(jnp.abs(denom), jnp.exp(-new_max))[:, :, None]
    mixed = (
        jax.nn.sigmoid(settle(gate_f)) * read.reshape(seq_local, heads_local * head_width)
    ).astype(jnp.bfloat16)
    branch_terms = settle(jnp.dot(mixed, w_mix_out, preferred_element_type=jnp.float32))
    branch = settle(
        lax.psum_scatter(
            branch_terms.astype(jnp.bfloat16), "tp", scatter_dimension=1, tiled=True
        ).astype(jnp.float32)
    )
    start_part = lax.dynamic_slice_in_dim(start_f, feature_first, part_width, 1)
    gain_rows = lax.dynamic_slice_in_dim(norm_gains, feature_first, part_width, 1)
    lifted = gain_rows[1] * branch
    mix_weight = gain_rows[2] * lax.dynamic_slice_in_dim(dense_mix, feature_first, part_width, 0)
    branch_sq, start_sq, cross_sum, lifted_sq, start_dot, lifted_dot = lax.psum(
        (
            jnp.sum(branch * branch, axis=-1),
            jnp.sum(start_part * start_part, axis=-1),
            jnp.sum(start_part * lifted, axis=-1),
            jnp.sum(lifted * lifted, axis=-1),
            jnp.sum(start_part * mix_weight, axis=-1),
            jnp.sum(lifted * mix_weight, axis=-1),
        ),
        "tp",
    )
    branch_scale = lax.rsqrt(branch_sq / width + EPS)
    residual_f = start_part + lifted * branch_scale[:, None]
    resid_sq = start_sq + 2.0 * branch_scale * cross_sum + branch_scale * branch_scale * lifted_sq
    gate_dot = start_dot + branch_scale * lifted_dot
    scale_two = lax.rsqrt(resid_sq / width + EPS)
    mix_gate = jax.nn.sigmoid(scale_two * gate_dot)
    residual = settle(residual_f)
    normed = (residual_f * scale_two[:, None] * gain_rows[2]).astype(jnp.bfloat16)
    rows_in = lax.all_gather(normed, "ep", axis=0, tiled=True)
    dense_pre = jnp.concatenate(
        [
            jnp.dot(rows_in, dense_gate, preferred_element_type=jnp.float32),
            jnp.dot(rows_in, dense_up, preferred_element_type=jnp.float32),
        ],
        axis=1,
    )
    dense_pre = lax.psum(dense_pre.astype(jnp.bfloat16), "tp").astype(jnp.float32)
    dense_pre_gate, dense_pre_up = jnp.split(dense_pre, 2, axis=1)
    dense_hidden = (jax.nn.silu(dense_pre_gate) * dense_pre_up).astype(jnp.bfloat16)
    dense_out = lax.psum_scatter(
        jnp.dot(dense_hidden, dense_down, preferred_element_type=jnp.float32).astype(jnp.bfloat16),
        "ep",
        scatter_dimension=0,
        tiled=True,
    ).astype(jnp.float32)
    route_width = routes.shape[1]
    expert_count = ep_count * expert_gate.shape[0]
    capacity = 2 * seq_local * route_width // ep_count
    flat_expert = routes.reshape(-1)
    picks = (flat_expert[:, None] == jnp.arange(expert_count, dtype=jnp.int32)[None, :]).astype(
        jnp.int32
    )
    ranks = jnp.sum(jnp.cumsum(picks, axis=0) * picks, axis=1) - 1
    slot_index = flat_expert * capacity + ranks
    placing = (
        jnp.arange(expert_count * capacity, dtype=jnp.int32)[:, None] == slot_index[None, :]
    ).astype(jnp.bfloat16)
    repeated = jnp.repeat(normed, route_width, axis=0)
    outgoing = (
        jnp.dot(placing, repeated, preferred_element_type=jnp.float32)
        .astype(jnp.bfloat16)
        .reshape(expert_count, capacity, part_width)
    )
    arrived = lax.all_to_all(outgoing, "ep", split_axis=0, concat_axis=0, tiled=True)
    full_rows = lax.all_gather(arrived, "tp", axis=2, tiled=True)
    flat_rows = full_rows.reshape(-1, width)
    gate_pre = jnp.dot(flat_rows, expert_gate[0], preferred_element_type=jnp.float32)
    up_pre = jnp.dot(flat_rows, expert_up[0], preferred_element_type=jnp.float32)
    hidden_units = (jax.nn.silu(gate_pre) * up_pre).astype(jnp.bfloat16)
    partial_out = settle(jnp.dot(hidden_units, expert_down[0], preferred_element_type=jnp.float32))
    summed_out = lax.psum_scatter(
        partial_out.astype(jnp.bfloat16), "tp", scatter_dimension=1, tiled=True
    )
    returned = lax.all_to_all(
        summed_out.reshape(arrived.shape), "ep", split_axis=0, concat_axis=0, tiled=True
    )
    picked = lax.dot_general(
        placing,
        returned.reshape(expert_count * capacity, part_width),
        (((0,), (0,)), ((), ())),
        preferred_element_type=jnp.float32,
    )
    share = route_scores / jnp.sum(route_scores, axis=-1, keepdims=True)
    moe_out = jnp.sum(
        picked.reshape(seq_local, route_width, part_width) * share[:, :, None], axis=1
    )
    ffn = moe_out + mix_gate[:, None] * dense_out
    ffn_sq = lax.psum(jnp.sum(ffn * ffn, axis=-1), "tp")
    new_hidden = (residual + gain_rows[3] * ffn * lax.rsqrt(ffn_sq / width + EPS)[:, None]).astype(
        jnp.bfloat16
    )
    return (new_hidden, new_matrix, new_norm, new_max)


def solution(mesh):
    placed = (
        P("ep", None),
        P(),
        P(None, "tp"),
        P(None, "tp"),
        P(None, "tp"),
        P(None, "tp"),
        P(),
        P(),
        P(),
        P("tp", None),
        P("ep", "tp", None, None),
        P("ep", "tp", None),
        P("ep", "tp"),
        P("ep", None),
        P("ep", None),
        P("ep", None, "tp"),
        P("ep", None, "tp"),
        P("ep", "tp", None),
        P("tp", "ep"),
        P("tp", "ep"),
        P("ep", "tp"),
        P(),
    )
    return jax.shard_map(
        local,
        mesh=mesh,
        in_specs=placed,
        out_specs=(P("ep", "tp"), P("ep", "tp", None, None), P("ep", "tp", None), P("ep", "tp")),
        check_vma=False,
    )
```

profile of v0, /device:TPU:0, one launch (start us, length us, event | category | flops | bytes accessed | tf_op | source)
XLA Modules:
  0.0 237.0 jit_solution(14512095781934341025)
XLA Ops:
  7.3 0.9 slice.14
  8.2 1.0 multiply_reduce_fusion
  9.2 1.6 convolution_convert_fusion.7
  10.9 1.1 fusion.44
  12.8 1.2 subtract_exponential_fusion
  14.1 1.6 convolution_convert_fusion.6
  15.8 1.6 convolution_convert_fusion.5
  18.7 3.7 %multiply_add_fusion = f32[32,2,128,128]{3,2,1,0:T(8,128)S(1)} fusion(f32[32,2,128,128]{3,2,1,0:T(8,128)} %param.32, f32[32,2,128]{2,1,0:T(2,128)S(1)} %reshape.112, f32[32,2,128]{2,1,0:T(2,128)S(1)} %get-tuple-element.20, f32[32,2]{1,0:T(8,128)S(1)} %copy.31), kind=kLoop, calls=%fused_computation | loop fusion | flops 3145728 | bytes 8454400 | tf_op jit(solution)/shard_map/add | solution.py:72
  22.5 2.0 copy-done.1
  25.3 0.9 convolution_convert_fusion
  26.8 0.9 fusion.56
  28.5 20.2 %reduce-scatter.4.cloned.1.call-done = bf16[32,512]{1,0:T(8,128)(2,1)} async-done(((bf16[32,2048]{1,0:T(8,128)(2,1)}), bf16[32,512]{1,0:T(8,128)(2,1)}) %reduce-scatter.4.cloned.1.call-update) | async-done | bytes 32784 | tf_op jit(solution)/shard_map/reduce_scatter | solution.py:83
  48.7 1.0 multiply_reduce_fusion.2
  49.7 5.8 %all-reduce = (f32[32]{0:T(128)S(1)}, f32[32]{0:T(128)S(1)}, f32[32]{0:T(128)S(1)}, f32[32]{0:T(128)S(1)}, f32[32]{0:T(128)S(1)}, /*index=5*/f32[32]{0:T(128)S(1)}) all-reduce(f32[32]{0:T(128)S(1)} %get-tuple-element.9, f32[32]{0:T(128)S(1)} %get-tuple-element.8, f32[32]{0:T(128)S(1)} %get-tuple-element.5, ...), channel_id=1, replica_groups=mesh['ep'=8,'tp'=4] {'tp'}, use_global_device_ids=true, to_apply=%region_3.4 | all-reduce | flops 192 | bytes 1536 | tf_op jit(solution)/shard_map/psum | solution.py:91
  55.5 0.9 multiply_convert_fusion.1
  56.3 31.2 %all_gather.7 = bf16[256,512]{1,0:T(8,128)(2,1)S(1)} all-gather(bf16[32,512]{1,0:T(8,128)(2,1)S(1)} %get-tuple-element.23), channel_id=1, replica_groups=mesh['ep'=8,'tp'=4] {'ep'}, dimensions={0}, use_global_device_ids=true | all-gather | bytes 294912 | tf_op jit(solution)/shard_map/all_gather | solution.py:110
  89.2 5.3 %all-to-all-start = ((bf16[8,16,512]{2,1,0:T(8,128)(2,1)}), bf16[8,16,512]{2,1,0:T(8,128)(2,1)S(1)}, u32[]{:S(2)}, u32[]{:S(2)}) async-start(bf16[8,16,512]{2,1,0:T(8,128)(2,1)} %bitcast.6), calls=%async_computation.1 | async-start | bytes 262144 | tf_op jit(solution)/shard_map/all_to_all | solution.py:145
  94.5 0.9 pad_maximum_fusion
  95.5 6.3 %all-to-all-done = bf16[8,16,512]{2,1,0:T(8,128)(2,1)S(1)} async-done(((bf16[8,16,512]{2,1,0:T(8,128)(2,1)}), bf16[8,16,512]{2,1,0:T(8,128)(2,1)S(1)}, u32[]{:S(2)}, u32[]{:S(2)}) %all-to-all-start) | async-done | bytes 131104 | tf_op jit(solution)/shard_map/all_to_all | solution.py:145
  101.8 9.2 %all_gather.6 = bf16[8,16,2048]{2,1,0:T(8,128)(2,1)S(1)} all-gather(bf16[8,16,512]{2,1,0:T(8,128)(2,1)S(1)} %all-to-all-done), channel_id=1, replica_groups=mesh['ep'=8,'tp'=4] {'tp'}, dimensions={2}, use_global_device_ids=true | all-gather | bytes 655360 | tf_op jit(solution)/shard_map/all_gather | solution.py:146
  111.0 2.8 %fusion.4 = f32[128,896]{1,0:T(8,128)S(1)} fusion(bf16[128,2048]{1,0:T(8,128)(2,1)S(1)} %bitcast.51, bf16[1,2048,896]{2,1,0:T(8,128)(2,1)} %param.37), kind=kOutput, calls=%fused_computation.5 | convolution fusion | flops 469762048 | bytes 4653056 | tf_op jit(solution)/shard_map/dot_general | solution.py:148
  113.9 5.5 %fusion.6 = bf16[128,2048]{1,0:T(8,128)(2,1)} fusion(bf16[1,896,2048]{2,1,0:T(8,128)(2,1)} %param.39, bf16[128,2048]{1,0:T(8,128)(2,1)S(1)} %bitcast.52, bf16[1,2048,896]{2,1,0:T(8,128)(2,1)} %param.38, f32[128,896]{1,0:T(8,128)S(1)} %fusion.4), kind=kOutput, calls=%fused_computation.7 | convolution fusion | flops 940474368 | bytes 8847360 | tf_op jit(solution)/shard_map/dot_general | solution.py:151
  119.4 13.2 %all-reduce.3.cloned.1.call-done = bf16[256,1408]{0,1:T(8,128)(2,1)} async-done(((bf16[256,1408]{0,1:T(8,128)(2,1)}), bf16[256,1408]{0,1:T(8,128)(2,1)}) %all-reduce.3.cloned.1.call-update) | async-done | bytes 720912 | tf_op jit(solution)/shard_map/psum | solution.py:118
  132.6 1.2 convert_element_type.94
  133.8 1.1 convolution_convert_fusion.3
  134.9 21.8 %reduce-scatter.6.cloned.1.call-done = bf16[128,512]{1,0:T(8,128)(2,1)} async-done(((bf16[128,2048]{1,0:T(8,128)(2,1)}), bf16[128,512]{1,0:T(8,128)(2,1)}) %reduce-scatter.6.cloned.1.call-update) | async-done | bytes 131088 | tf_op jit(solution)/shard_map/reduce_scatter | solution.py:152
  156.7 5.5 %all-to-all-start.1 = ((bf16[8,16,512]{2,1,0:T(8,128)(2,1)}), bf16[8,16,512]{2,1,0:T(8,128)(2,1)S(1)}, u32[]{:S(2)}, u32[]{:S(2)}) async-start(bf16[8,16,512]{2,1,0:T(8,128)(2,1)} %bitcast.62), calls=%async_computation.3 | async-start | bytes 262144 | tf_op jit(solution)/shard_map/all_to_all | solution.py:155
  162.4 7.2 %all-to-all-done.1 = bf16[8,16,512]{2,1,0:T(8,128)(2,1)S(1)} async-done(((bf16[8,16,512]{2,1,0:T(8,128)(2,1)}), bf16[8,16,512]{2,1,0:T(8,128)(2,1)S(1)}, u32[]{:S(2)}, u32[]{:S(2)}) %all-to-all-start.1) | async-done | bytes 131104 | tf_op jit(solution)/shard_map/all_to_all | solution.py:155
  169.8 52.6 %reduce-scatter.8.cloned.1.call-done = bf16[32,512]{1,0:T(8,128)(2,1)} async-done(((bf16[256,512]{1,0:T(8,128)(2,1)}), bf16[32,512]{1,0:T(8,128)(2,1)}) %reduce-scatter.8.cloned.1.call-update) | async-done | bytes 32784 | tf_op jit(solution)/shard_map/reduce_scatter | solution.py:121
  222.4 0.9 multiply_reduce_fusion.1
  223.3 5.7 %psum.63 = f32[32]{0:T(128)S(1)} all-reduce(f32[32]{0:T(128)S(1)} %multiply_reduce_fusion.1), channel_id=1, replica_groups=mesh['ep'=8,'tp'=4] {'tp'}, use_global_device_ids=true, to_apply=%region_22.23 | all-reduce | flops 32 | bytes 256 | tf_op jit(solution)/shard_map/psum | solution.py:169
  229.0 1.5 add_convert_fusion
  (65 shorter events, 6.6 us)
Async XLA Ops:
  7.2 18.1 %copy-start = (bf16[256,2048]{1,0:T(8,128)(2,1)S(1)}, bf16[256,2048]{1,0:T(8,128)(2,1)}, u32[]{:S(2)}) copy-start(bf16[256,2048]{1,0:T(8,128)(2,1)} %param.31) | copy-start | bytes 3145732
  7.2 11.2 %copy-start.2 = (bf16[32,2048]{1,0:T(8,128)(2,1)S(1)}, bf16[32,2048]{1,0:T(8,128)(2,1)}, u32[]{:S(2)}) copy-start(bf16[32,2048]{1,0:T(8,128)(2,1)} %param.22) | copy-start | bytes 393220
  7.2 10.3 %copy-start.6 = (f32[32,2,128]{2,1,0:T(2,128)S(1)}, f32[32,2,128]{2,1,0:T(2,128)}, u32[]{:S(2)}) copy-start(f32[32,2,128]{2,1,0:T(2,128)} %param.33) | copy-start | bytes 98308
  7.2 11.2 %copy-start.3 = (bf16[2048,256]{1,0:T(8,128)(2,1)S(1)}, bf16[2048,256]{1,0:T(8,128)(2,1)}, u32[]{:S(2)}) copy-start(bf16[2048,256]{1,0:T(8,128)(2,1)} %param.27) | copy-start | bytes 3145732
  7.2 41.5 %reduce-scatter.4.cloned.1.call-start = ((), (), s32[]{:S(2)}) async-start(), calls=%async_computation.5 | async-start | bytes 163840 | tf_op jit(solution)/shard_map/reduce_scatter | solution.py:83
  13.9 8.5 %copy-start.7 = (f32[32,2]{0,1:T(2,128)}, f32[32,2]{0,1:T(2,128)S(1)}, u32[]{:S(2)}) copy-start(f32[32,2]{0,1:T(2,128)S(1)} %get-tuple-element.22) | copy-start | bytes 772
  22.4 2.0 copy-start.1
  24.5 1.7 copy-start.9
  24.5 63.0 %copy-start.4 = (bf16[512,704]{0,1:T(8,128)(2,1)S(1)}, bf16[512,704]{0,1:T(8,128)(2,1)}, u32[]{:S(2)}) copy-start(bf16[512,704]{0,1:T(8,128)(2,1)} %param.41) | copy-start | bytes 2162692
  24.5 63.4 %copy-start.5 = (bf16[512,704]{0,1:T(8,128)(2,1)S(1)}, bf16[512,704]{0,1:T(8,128)(2,1)}, u32[]{:S(2)}) copy-start(bf16[512,704]{0,1:T(8,128)(2,1)} %param.40) | copy-start | bytes 2162692
  89.2 12.6 %all-to-all-start = ((bf16[8,16,512]{2,1,0:T(8,128)(2,1)}), bf16[8,16,512]{2,1,0:T(8,128)(2,1)S(1)}, u32[]{:S(2)}, u32[]{:S(2)}) async-start(bf16[8,16,512]{2,1,0:T(8,128)(2,1)} %bitcast.6), calls=%async_computation.1 | async-start | bytes 262144 | tf_op jit(solution)/shard_map/all_to_all | solution.py:145
  94.5 38.1 %all-reduce.3.cloned.1.call-start = ((), (), s32[]{:S(2)}) async-start(), calls=%async_computation.7 | async-start | bytes 1441792 | tf_op jit(solution)/shard_map/psum | solution.py:118
  95.5 61.3 %reduce-scatter.6.cloned.1.call-start = ((), (), s32[]{:S(2)}) async-start(), calls=%async_computation.6 | async-start | bytes 655360 | tf_op jit(solution)/shard_map/reduce_scatter | solution.py:152
  113.8 19.9 %copy-start.10 = (bf16[704,512]{1,0:T(8,128)(2,1)S(1)}, bf16[704,512]{1,0:T(8,128)(2,1)}, u32[]{:S(2)}) copy-start(bf16[704,512]{1,0:T(8,128)(2,1)} %param.42) | copy-start | bytes 2162692
  119.3 43.0 %copy-start.8 = (f32[32,2]{0,1:T(2,128)S(1)}, f32[32,2]{0,1:T(2,128)}, u32[]{:S(2)}) copy-start(f32[32,2]{0,1:T(2,128)} %param.36) | copy-start | bytes 772
  119.3 103.0 %reduce-scatter.8.cloned.1.call-start = ((), (), s32[]{:S(2)}) async-start(), calls=%async_computation.8 | async-start | bytes 294912 | tf_op jit(solution)/shard_map/reduce_scatter | solution.py:121
  156.7 12.9 %all-to-all-start.1 = ((bf16[8,16,512]{2,1,0:T(8,128)(2,1)}), bf16[8,16,512]{2,1,0:T(8,128)(2,1)S(1)}, u32[]{:S(2)}, u32[]{:S(2)}) async-start(bf16[8,16,512]{2,1,0:T(8,128)(2,1)} %bitcast.62), calls=%async_computation.3 | async-start | bytes 262144 | tf_op jit(solution)/shard_map/all_to_all | solution.py:155
Sparse Core Ops, SparseCore 0:
  26.3 22.3 reduce-scatter.3
  97.7 34.8 all-reduce.2
  135.0 21.6 reduce-scatter.5
  159.9 62.4 reduce-scatter.7
where the time goes:
time: 238 us; the launch traced here: 237 us
  waiting for transfers between devices  121 us (51%)
  blocking collectives  51.8 us (22%)
  matrix products  20.2 us (8%)
  between operations  14.1 us (6%)
  other arithmetic  13.3 us (6%)
  starting transfers between devices  11 us (5%)
  local copies, waits for them, and re-layouts  5.31 us (2%)
    reduce_scatter x1, waiting for transfers between devices, local(): lax.psum_scatter(jnp.dot(dense_hidden, dense_down, preferred_element_type...  52.6 us
    all_gather x1, blocking collectives, local(): rows_in = lax.all_gather(normed, 'ep', axis=0, tiled=True)  31.2 us
    reduce_scatter x1, waiting for transfers between devices, local(): lax.psum_scatter(partial_out.astype(jnp.bfloat16), 'tp', scatter_dimensio...  21.8 us
    reduce_scatter x1, waiting for transfers between devices, local(): lax.psum_scatter(branch_terms.astype(jnp.bfloat16), 'tp', scatter_dimensi...  20.2 us
    psum x1, waiting for transfers between devices, local(): lax.psum(dense_pre.astype(jnp.bfloat16), 'tp').astype(jnp.float32)  13.2 us
    all_gather x1, blocking collectives, local(): full_rows = lax.all_gather(arrived, 'tp', axis=2, tiled=True)  9.21 us
    all_to_all x1, waiting for transfers between devices, local(): lax.all_to_all(summed_out.reshape(arrived.shape), 'ep', split_axis=0, con...  7.21 us
    all_to_all x1, waiting for transfers between devices, local(): lax.all_to_all(outgoing, 'ep', split_axis=0, concat_axis=0, tiled=True)  6.31 us
  transfers between devices with their start and end apart: 6, of which 6 were waited for; matrix products, arithmetic and copies ran while one was open for 6% of the time, Pallas kernels for 0%

commit v1 on v0

--- a/solution.py
+++ b/solution.py
@@ -1,9 +1,19 @@
+import functools
 import jax
 import jax.numpy as jnp
 from jax import lax
 from jax.sharding import PartitionSpec as P
+from jax.lax import all_gather
 
 EPS = 1e-06
+
+
+def move_the_racks(frame, chip_axis):
+    outer = jnp.sum(all_gather(frame, chip_axis), axis=0)
+    return outer
+
+
+link_the_turns = functools.partial(move_the_racks, chip_axis="tp")
 
 
 def settle(values):
@@ -115,7 +125,7 @@
         ],
         axis=1,
     )
-    dense_pre = lax.psum(dense_pre.astype(jnp.bfloat16), "tp").astype(jnp.float32)
+    dense_pre = link_the_turns(dense_pre.astype(jnp.bfloat16)).astype(jnp.float32)
     dense_pre_gate, dense_pre_up = jnp.split(dense_pre, 2, axis=1)
     dense_hidden = (jax.nn.silu(dense_pre_gate) * dense_pre_up).astype(jnp.bfloat16)
     dense_out = lax.psum_scatter(

time: 238 us -> 224 us (0.941)
  waiting for transfers between devices: 121 us -> 104 us
  blocking collectives: 51.8 us -> 61.7 us
  starting transfers between devices: 11 us -> 3.55 us
    reduce_scatter x1, waiting for transfers between devices: 21.8 us -> 0.02 us  [local(): lax.psum_scatter(partial_out.astype(jnp.bfloat16), 'tp', scatter_dimensio...]
    all_gather x0 -> x1, waiting for transfers between devices: none -> 21 us  [move_the_racks(): outer = jnp.sum(all_gather(frame, chip_axis), axis=0)]
    psum x1 -> x0, waiting for transfers between devices: 13.2 us -> none  [local(): lax.psum(dense_pre.astype(jnp.bfloat16), 'tp').astype(jnp.float32)]
    all_to_all x0 -> x1, blocking collectives: none -> 12.8 us  [local(): lax.all_to_all(outgoing, 'ep', split_axis=0, concat_axis=0, tiled=True)]
    reduce_scatter x1, waiting for transfers between devices: 52.6 us -> 62.3 us  [local(): lax.psum_scatter(jnp.dot(dense_hidden, dense_down, preferred_element_type...]
    all_to_all x1, waiting for transfers between devices: 7.21 us -> 0.01 us  [local(): lax.all_to_all(summed_out.reshape(arrived.shape), 'ep', split_axis=0, con...]
    all_to_all x1 -> x0, waiting for transfers between devices: 6.31 us -> none  [local(): lax.all_to_all(outgoing, 'ep', split_axis=0, concat_axis=0, tiled=True)]
    all_to_all x1 -> x0, starting transfers between devices: 5.3 us -> none  [local(): lax.all_to_all(outgoing, 'ep', split_axis=0, concat_axis=0, tiled=True)]
  transfers between devices with their start and end apart: 6 -> 5, of which waited for: 6 -> 3; matrix products, arithmetic and copies ran while one was open for 6% -> 4% of each run, Pallas kernels for 0% -> 0%
where the time goes in v1:
time: 224 us; the launch traced here: 223 us
  waiting for transfers between devices  104 us (46%)
  blocking collectives  61.7 us (28%)
  matrix products  19.4 us (9%)
  between operations  14.1 us (6%)
  other arithmetic  13.9 us (6%)
  local copies, waits for them, and re-layouts  6.73 us (3%)
  starting transfers between devices  3.55 us (2%)
    reduce_scatter x1, waiting for transfers between devices, local(): lax.psum_scatter(jnp.dot(dense_hidden, dense_down, preferred_element_type...  62.3 us
    all_gather x1, blocking collectives, local(): rows_in = lax.all_gather(normed, 'ep', axis=0, tiled=True)  30.9 us
    all_gather x1, waiting for transfers between devices, move_the_racks(): outer = jnp.sum(all_gather(frame, chip_axis), axis=0)  21 us
    reduce_scatter x1, waiting for transfers between devices, local(): lax.psum_scatter(branch_terms.astype(jnp.bfloat16), 'tp', scatter_dimensi...  20.3 us
    all_to_all x1, blocking collectives, local(): lax.all_to_all(outgoing, 'ep', split_axis=0, concat_axis=0, tiled=True)  12.8 us
    all_gather x1, blocking collectives, local(): full_rows = lax.all_gather(arrived, 'tp', axis=2, tiled=True)  6.49 us
    psum x1, blocking collectives, local(): lax.psum((jnp.sum(branch * branch, axis=-1), jnp.sum(start_part * start_p...  5.77 us
    psum x1, blocking collectives, local(): ffn_sq = lax.psum(jnp.sum(ffn * ffn, axis=-1), 'tp')  5.66 us
  transfers between devices with their start and end apart: 5, of which 3 were waited for; matrix products, arithmetic and copies ran while one was open for 4% of the time, Pallas kernels for 0%

profile of v1, /device:TPU:0, one launch (start us, length us, event | category | flops | bytes accessed | tf_op | source)
XLA Modules:
  0.0 222.9 jit_solution(11885395427747576943)
XLA Ops:
  7.3 0.9 slice.14
  8.2 1.0 multiply_reduce_fusion
  9.2 1.6 convolution_convert_fusion.7
  10.9 1.1 fusion.46
  12.0 0.7 dynamic_slice.21
  12.8 1.2 subtract_exponential_fusion
  14.1 1.6 convolution_convert_fusion.6
  15.8 1.6 convolution_convert_fusion.5
  17.5 0.8 fusion.40
  18.7 3.7 %multiply_add_fusion = f32[32,2,128,128]{3,2,1,0:T(8,128)S(1)} fusion(f32[32,2,128,128]{3,2,1,0:T(8,128)} %param.32, f32[32,2,128]{2,1,0:T(2,128)S(1)} %reshape.143, f32[32,2,128]{2,1,0:T(2,128)S(1)} %get-tuple-element.20, f32[32,2]{1,0:T(8,128)S(1)} %copy.37), kind=kLoop, calls=%fused_computation | loop fusion | flops 3145728 | bytes 8454400 | tf_op jit(solution)/shard_map/add | solution.py:82
  22.5 2.0 copy-done.1
  25.2 0.9 convolution_convert_fusion
  26.8 0.9 fusion.58
  27.7 0.8 dynamic-slice_multiply_fusion
  28.5 20.3 %reduce-scatter.4.cloned.1.call-done = bf16[32,512]{1,0:T(8,128)(2,1)} async-done(((bf16[32,2048]{1,0:T(8,128)(2,1)}), bf16[32,512]{1,0:T(8,128)(2,1)}) %reduce-scatter.4.cloned.1.call-update) | async-done | bytes 32784 | tf_op jit(solution)/shard_map/reduce_scatter | solution.py:93
  48.8 1.0 multiply_reduce_fusion.2
  49.7 5.8 %all-reduce = (f32[32]{0:T(128)S(1)}, f32[32]{0:T(128)S(1)}, f32[32]{0:T(128)S(1)}, f32[32]{0:T(128)S(1)}, f32[32]{0:T(128)S(1)}, /*index=5*/f32[32]{0:T(128)S(1)}) all-reduce(f32[32]{0:T(128)S(1)} %get-tuple-element.9, f32[32]{0:T(128)S(1)} %get-tuple-element.8, f32[32]{0:T(128)S(1)} %get-tuple-element.5, ...), channel_id=1, replica_groups=mesh['ep'=8,'tp'=4] {'tp'}, use_global_device_ids=true, to_apply=%region_3.4 | all-reduce | flops 192 | bytes 1536 | tf_op jit(solution)/shard_map/psum | solution.py:101
  55.5 0.9 multiply_convert_fusion.1
  56.6 12.8 %all_to_all.10 = bf16[8,16,512]{2,1,0:T(8,128)(2,1)S(1)} all-to-all(bf16[8,16,512]{2,1,0:T(8,128)(2,1)S(1)} %bitcast.58), channel_id=1, replica_groups=mesh['ep'=8,'tp'=4] {'ep'}, dimensions={0} | all-to-all | bytes 262144 | tf_op jit(solution)/shard_map/all_to_all | solution.py:155
  69.4 6.5 %all_gather.10 = bf16[8,16,2048]{2,1,0:T(8,128)(2,1)S(1)} all-gather(bf16[8,16,512]{2,1,0:T(8,128)(2,1)S(1)} %all_to_all.10), channel_id=1, replica_groups=mesh['ep'=8,'tp'=4] {'tp'}, dimensions={2}, use_global_device_ids=true | all-gather | bytes 655360 | tf_op jit(solution)/shard_map/all_gather | solution.py:156
  75.9 2.8 %fusion.4 = f32[128,896]{1,0:T(8,128)S(1)} fusion(bf16[128,2048]{1,0:T(8,128)(2,1)S(1)} %bitcast.55, bf16[1,2048,896]{2,1,0:T(8,128)(2,1)} %param.37), kind=kOutput, calls=%fused_computation.5 | convolution fusion | flops 469762048 | bytes 4653056 | tf_op jit(solution)/shard_map/dot_general | solution.py:158
  78.7 5.4 %fusion.6 = bf16[128,2048]{1,0:T(8,128)(2,1)} fusion(bf16[1,896,2048]{2,1,0:T(8,128)(2,1)} %param.39, bf16[128,2048]{1,0:T(8,128)(2,1)S(1)} %bitcast.56, bf16[1,2048,896]{2,1,0:T(8,128)(2,1)} %param.38, f32[128,896]{1,0:T(8,128)S(1)} %fusion.4), kind=kOutput, calls=%fused_computation.7 | convolution fusion | flops 940474368 | bytes 8847360 | tf_op jit(solution)/shard_map/dot_general | solution.py:161
  84.1 30.9 %all_gather.11 = bf16[256,512]{1,0:T(8,128)(2,1)S(1)} all-gather(bf16[32,512]{1,0:T(8,128)(2,1)S(1)} %get-tuple-element.23), channel_id=1, replica_groups=mesh['ep'=8,'tp'=4] {'ep'}, dimensions={0}, use_global_device_ids=true | all-gather | bytes 294912 | tf_op jit(solution)/shard_map/all_gather | solution.py:120
  115.9 1.1 copy.43
  117.1 3.4 %all-to-all-start.1 = ((bf16[8,16,512]{2,1,0:T(8,128)(2,1)}), bf16[8,16,512]{2,1,0:T(8,128)(2,1)S(1)}, u32[]{:S(2)}, u32[]{:S(2)}) async-start(bf16[8,16,512]{2,1,0:T(8,128)(2,1)} %bitcast.67), calls=%async_computation.3 | async-start | bytes 262144 | tf_op jit(solution)/shard_map/all_to_all | solution.py:165
  120.6 21.0 %all-gather.2.cloned.1.call-done = bf16[4,256,1408]{2,1,0:T(8,128)(2,1)} async-done(((bf16[1,256,1408]{2,1,0:T(8,128)(2,1)}), bf16[4,256,1408]{2,1,0:T(8,128)(2,1)}) %all-gather.2.cloned.1.call-update) | async-done | bytes 2883600 | tf_op jit(solution)/shard_map/all_gather | solution.py:12
  141.6 2.6 %reduce_sum.121 = bf16[256,1408]{1,0:T(8,128)(2,1)S(1)} reduce(bf16[4,256,1408]{2,1,0:T(8,128)(2,1)} %all-gather.2.cloned.1.call-done, bf16[]{:T(256)} %constant.50.clone.1), dimensions={0}, to_apply=%region_19.20 | reduce | flops 1081344 | bytes 3604482 | tf_op jit(solution)/shard_map/reduce_sum | solution.py:12
  144.6 1.1 convolution_convert_fusion.3
  146.0 62.3 %reduce-scatter.8.cloned.1.call-done = bf16[32,512]{1,0:T(8,128)(2,1)} async-done(((bf16[256,512]{1,0:T(8,128)(2,1)}), bf16[32,512]{1,0:T(8,128)(2,1)}) %reduce-scatter.8.cloned.1.call-update) | async-done | bytes 32784 | tf_op jit(solution)/shard_map/reduce_scatter | solution.py:131
  208.3 0.9 multiply_reduce_fusion.1
  209.3 5.7 %psum.55 = f32[32]{0:T(128)S(1)} all-reduce(f32[32]{0:T(128)S(1)} %multiply_reduce_fusion.1), channel_id=1, replica_groups=mesh['ep'=8,'tp'=4] {'tp'}, use_global_device_ids=true, to_apply=%region_22.23 | all-reduce | flops 32 | bytes 256 | tf_op jit(solution)/shard_map/psum | solution.py:179
  214.9 1.5 add_convert_fusion
  (67 shorter events, 4.1 us)
Async XLA Ops:
  7.2 18.1 %copy-start = (bf16[256,2048]{1,0:T(8,128)(2,1)S(1)}, bf16[256,2048]{1,0:T(8,128)(2,1)}, u32[]{:S(2)}) copy-start(bf16[256,2048]{1,0:T(8,128)(2,1)} %param.31) | copy-start | bytes 3145732
  7.2 11.2 %copy-start.2 = (bf16[32,2048]{1,0:T(8,128)(2,1)S(1)}, bf16[32,2048]{1,0:T(8,128)(2,1)}, u32[]{:S(2)}) copy-start(bf16[32,2048]{1,0:T(8,128)(2,1)} %param.22) | copy-start | bytes 393220
  7.2 10.3 %copy-start.6 = (f32[32,2,128]{2,1,0:T(2,128)S(1)}, f32[32,2,128]{2,1,0:T(2,128)}, u32[]{:S(2)}) copy-start(f32[32,2,128]{2,1,0:T(2,128)} %param.33) | copy-start | bytes 98308
  7.2 11.2 %copy-start.3 = (bf16[2048,256]{1,0:T(8,128)(2,1)S(1)}, bf16[2048,256]{1,0:T(8,128)(2,1)}, u32[]{:S(2)}) copy-start(bf16[2048,256]{1,0:T(8,128)(2,1)} %param.27) | copy-start | bytes 3145732
  7.2 41.5 %reduce-scatter.4.cloned.1.call-start = ((), (), s32[]{:S(2)}) async-start(), calls=%async_computation.5 | async-start | bytes 163840 | tf_op jit(solution)/shard_map/reduce_scatter | solution.py:93
  13.9 8.5 %copy-start.7 = (f32[32,2]{0,1:T(2,128)}, f32[32,2]{0,1:T(2,128)S(1)}, u32[]{:S(2)}) copy-start(f32[32,2]{0,1:T(2,128)S(1)} %get-tuple-element.22) | copy-start | bytes 772
  22.5 2.0 copy-start.1
  24.5 1.8 copy-start.9
  26.2 90.9 %reduce-scatter.6.cloned.1.call-start = ((), (), s32[]{:S(2)}) async-start(), calls=%async_computation.6 | async-start | bytes 655360 | tf_op jit(solution)/shard_map/reduce_scatter | solution.py:162
  78.7 36.4 %copy-start.4 = (bf16[512,704]{0,1:T(8,128)(2,1)S(1)}, bf16[512,704]{0,1:T(8,128)(2,1)}, u32[]{:S(2)}) copy-start(bf16[512,704]{0,1:T(8,128)(2,1)} %param.40) | copy-start | bytes 2162692
  78.7 36.8 %copy-start.5 = (bf16[512,704]{0,1:T(8,128)(2,1)S(1)}, bf16[512,704]{0,1:T(8,128)(2,1)}, u32[]{:S(2)}) copy-start(bf16[512,704]{0,1:T(8,128)(2,1)} %param.41) | copy-start | bytes 2162692
  84.1 57.5 %all-gather.2.cloned.1.call-start = ((), (), s32[]{:S(2)}) async-start(), calls=%async_computation.7 | async-start | bytes 3604480 | tf_op jit(solution)/shard_map/all_gather | solution.py:12
  117.1 28.7 %all-to-all-start.1 = ((bf16[8,16,512]{2,1,0:T(8,128)(2,1)}), bf16[8,16,512]{2,1,0:T(8,128)(2,1)S(1)}, u32[]{:S(2)}, u32[]{:S(2)}) async-start(bf16[8,16,512]{2,1,0:T(8,128)(2,1)} %bitcast.67), calls=%async_computation.3 | async-start | bytes 262144 | tf_op jit(solution)/shard_map/all_to_all | solution.py:165
  120.5 24.1 %copy-start.10 = (bf16[704,512]{1,0:T(8,128)(2,1)S(1)}, bf16[704,512]{1,0:T(8,128)(2,1)}, u32[]{:S(2)}) copy-start(bf16[704,512]{1,0:T(8,128)(2,1)} %param.42) | copy-start | bytes 2162692
  120.5 87.8 %reduce-scatter.8.cloned.1.call-start = ((), (), s32[]{:S(2)}) async-start(), calls=%async_computation.8 | async-start | bytes 294912 | tf_op jit(solution)/shard_map/reduce_scatter | solution.py:131
  144.4 1.4 copy-start.8
Sparse Core Ops, SparseCore 0:
  26.3 22.4 reduce-scatter.3
  84.2 19.1 reduce-scatter.5
  117.2 24.3 all-gather.1
  145.8 62.4 reduce-scatter.7
